TPU v7x, 32 devices: a whole 2x2x4 slice. The times are simulated.
32 devices in a mesh: ep: 8 (over z, x), tp: 4 (over y, core).
Axes of the slice: x: 2, y: 2, z: 4, core: 2. Of those that a mesh axis runs over, the one named last changes fastest.
Arguments:
- tokens: bfloat16 [1024, 1024], P('ep', 'tp'), may hold values from -6 to 6
- cotangent: bfloat16 [1024, 1024], P('ep', 'tp'), may hold values from -4 to 4
- routes: int32 [1024, 2], P('ep'), may hold values from 0 to 7, all different within a row; in each aligned block of 128 rows (0 to 127, 128 to 255, ...) at most 40 rows name the same one
- route_weights: bfloat16 [1024, 2], P('ep'), may hold values from 0.099609375 to 0.8984375
- w_gate: bfloat16 [8, 1024, 2816], P('ep', None, 'tp'), may hold values from -0.1875 to 0.1875
- w_up: bfloat16 [8, 1024, 2816], P('ep', None, 'tp'), may hold values from -0.1875 to 0.1875
- w_down: bfloat16 [8, 2816, 1024], P('ep', 'tp'), may hold values from -0.109375 to 0.109375
- dense_weight: bfloat16 [1024, 1024], P('tp', 'ep'), may hold values from -0.25 to 0.25
- mix_gate: float32 [1024], replicated, may hold values from 0.1 to 1.9
Outputs:
- token_grad: bfloat16 [1024, 1024], P('ep', 'tp')
- route_grad: float32 [1024, 2], P('ep')
- gate_grad: bfloat16 [8, 1024, 2816], P('ep', None, 'tp')
- up_grad: bfloat16 [8, 1024, 2816], P('ep', None, 'tp')
- down_grad: bfloat16 [8, 2816, 1024], P('ep', 'tp')
- dense_grad: float32 [1024, 1024], P('tp', 'ep')
- mix_grad: float32 [1024], replicated
Inputs may be any that keep to these rules, and one draw needn't show every extreme that they name: `routes`: each row names 2 different experts. In the rows of one index of ep (aligned blocks of 128 rows) no expert is named by more than 40 rows, a bound that some block reaches.
All inputs are finite; a program needn't handle non-finite values.
Results may differ from a plain program's by a relative error of at most 0.0065.
Values may be sent and summed in bfloat16 or wider, within the bound.
A program may use at most 64 MiB of HBM per device.

v0:
```python
import jax
import jax.numpy as jnp
from jax import lax
from jax.sharding import PartitionSpec as P

FF = 2816
BF = jnp.bfloat16
F32 = jnp.float32


def spread(values, group_size):
    experts = values.shape[0]
    copies = jnp.broadcast_to(values[:, None], (experts, group_size) + values.shape[1:])
    return copies.reshape((experts * group_size,) + values.shape[1:])


def swap(values, axis):
    return lax.all_to_all(values, axis, split_axis=0, concat_axis=0, tiled=True)


def local(tokens, cotangent, routes, route_weights, w_gate, w_up, w_down, dense_weight, mix_gate):
    tp_count = lax.axis_size("tp")
    ep_count = lax.axis_size("ep")
    slice_width = w_gate.shape[2]
    group_size = FF // (slice_width * tp_count)
    experts = ep_count // group_size
    token_count, top_count = routes.shape
    width_part = tokens.shape[1]
    width = width_part * tp_count
    capacity = 5 * token_count * top_count // (4 * experts)
    slots = experts * capacity
    rows_here = ep_count * capacity
    expert_ids = jnp.arange(experts, dtype=jnp.int32)
    named = routes[:, :, None] == expert_ids[None, None, :]
    member = jnp.any(named, axis=1)
    token_ids = jnp.arange(token_count, dtype=jnp.int32)
    before = (token_ids[:, None] > token_ids[None, :]).astype(BF)
    rank = jnp.dot(before, member.astype(BF), preferred_element_type=F32)
    weight_of = jnp.sum(jnp.where(named, route_weights.astype(F32)[:, :, None], 0.0), axis=1)
    slot_ids = jnp.arange(capacity, dtype=jnp.int32).astype(F32)
    rank_t = jnp.where(member, rank, -1.0).T
    hit = rank_t[:, None, :] == slot_ids[None, :, None]
    dispatch = hit.astype(BF).reshape(slots, token_count)
    slot_weight = jnp.sum(jnp.where(hit, weight_of.T[:, None, :], 0.0), axis=2).astype(BF)

    def pick(values):
        taken = jnp.dot(dispatch, values, preferred_element_type=F32).astype(BF)
        return spread(taken.reshape(experts, capacity, values.shape[1]), group_size)

    rows_part = swap(pick(tokens), "ep")
    grads_full = lax.all_gather(cotangent, "tp", axis=1, tiled=True)
    lanes = jnp.broadcast_to(spread(slot_weight, group_size)[:, :, None], (ep_count, capacity, 128))
    arrived = swap(jnp.concatenate([pick(grads_full), lanes], axis=2), "ep")
    arrived = arrived.reshape(rows_here, width + 128)
    grads_in, weight_col = (arrived[:, :width], arrived[:, width : width + 1].astype(F32))
    rows_in = lax.all_gather(rows_part.reshape(rows_here, width_part), "tp", axis=1, tiled=True)
    contract_rows = (((0,), (0,)), ((), ()))
    contract_cols = (((1,), (1,)), ((), ()))
    dense_cols = dense_weight.shape[1]
    scaled = (mix_gate[None, :] * grads_full.astype(F32)).astype(BF)
    product = lax.dot_general(tokens, scaled, contract_rows, preferred_element_type=F32).astype(BF)
    product = product.reshape(width_part, ep_count, dense_cols).transpose(1, 0, 2)
    copies = jnp.broadcast_to(dense_weight[None], (ep_count,) + dense_weight.shape)
    outgoing, _ = lax.optimization_barrier((jnp.concatenate([copies, product], axis=1), arrived))
    met = swap(outgoing, "ep")
    gathered, shares = (met[:, :width_part], met[:, width_part:])
    dense_grad = jnp.sum(shares.astype(F32), axis=0) * (1.0 / ep_count)
    gate_matrix = w_gate[0]
    up_matrix = w_up[0]
    down_matrix = w_down[0]
    pre_gate = jnp.dot(rows_in, gate_matrix, preferred_element_type=F32)
    pre_up = jnp.dot(rows_in, up_matrix, preferred_element_type=F32)
    sigmoid_gate = jax.nn.sigmoid(pre_gate)
    activated = pre_gate * sigmoid_gate
    hidden = activated * pre_up
    hidden_bf = hidden.astype(BF)
    projected = lax.dot_general(grads_in, down_matrix, contract_cols, preferred_element_type=F32)
    route_part = jnp.sum(hidden_bf.astype(F32) * projected, axis=1)
    hidden_grad = weight_col * projected
    d_gate = (hidden_grad * pre_up * sigmoid_gate * (1.0 + pre_gate * (1.0 - sigmoid_gate))).astype(
        BF
    )
    d_up = (hidden_grad * activated).astype(BF)
    weighted = (weight_col * hidden).astype(BF)
    partial_value = (
        lax.dot_general(d_gate, gate_matrix, contract_cols, preferred_element_type=F32)
        + lax.dot_general(d_up, up_matrix, contract_cols, preferred_element_type=F32)
    ).astype(BF)
    mixed = lax.all_to_all(partial_value, "tp", split_axis=1, concat_axis=0, tiled=True)
    column_sum = jnp.sum(mixed.reshape(tp_count, rows_here, -1).astype(F32), axis=0).astype(BF)
    returned = swap(column_sum.reshape(ep_count, capacity, width_part), "ep")
    moment = lax.dot_general(tokens, grads_full, contract_rows, preferred_element_type=F32)
    moment = moment.reshape(width_part, ep_count, dense_cols)
    gain = jnp.sum(gathered.astype(F32) * moment.transpose(1, 0, 2), axis=1).reshape(1, width)
    gain, route_part, _ = lax.optimization_barrier((gain, route_part, mixed))
    devices = ep_count * tp_count
    route_rows = jnp.broadcast_to(
        route_part.reshape(ep_count, 1, capacity), (ep_count, tp_count, capacity)
    ).reshape(devices, capacity)
    packed = jnp.concatenate([jnp.broadcast_to(gain, (devices, width)), route_rows], axis=1)
    small = swap(packed[:, None, :], ("ep", "tp")).reshape(devices, width + capacity)
    mix_grad = jnp.sum(small[:, :width], axis=0) * (1.0 / ep_count)
    slot_route = jnp.sum(small[:, width:].reshape(experts, group_size * tp_count, capacity), axis=1)
    expert_route = jnp.sum(jnp.where(hit, slot_route[:, :, None], 0.0), axis=1).T
    route_grad = jnp.sum(jnp.where(named, expert_route[:, None, :], 0.0), axis=2)
    gate_grad = lax.dot_general(rows_in, d_gate, contract_rows, preferred_element_type=F32)
    up_grad = lax.dot_general(rows_in, d_up, contract_rows, preferred_element_type=F32)
    down_grad = lax.dot_general(weighted, grads_in, contract_rows, preferred_element_type=F32)
    back = returned.reshape(experts, group_size, capacity, width_part)
    combine = jnp.broadcast_to(hit[:, None], (experts, group_size) + hit.shape[1:]).astype(BF)
    expert_grad = lax.dot_general(
        combine.reshape(rows_here, token_count),
        back.reshape(rows_here, width_part),
        contract_rows,
        preferred_element_type=F32,
    )
    whole_weight = gathered.transpose(1, 0, 2).reshape(width_part, width)
    dense_dx = lax.dot_general(scaled, whole_weight, contract_cols, preferred_element_type=F32)
    token_grad = (expert_grad + dense_dx).astype(BF)
    return (
        token_grad,
        route_grad,
        gate_grad.astype(BF)[None],
        up_grad.astype(BF)[None],
        down_grad.astype(BF)[None],
        dense_grad,
        mix_grad,
    )


def solution(mesh):
    return jax.shard_map(
        local,
        mesh=mesh,
        in_specs=(
            P("ep", "tp"),
            P("ep", "tp"),
            P("ep", None),
            P("ep", None),
            P("ep", None, "tp"),
            P("ep", None, "tp"),
            P("ep", "tp", None),
            P("tp", "ep"),
            P(),
        ),
        out_specs=(
            P("ep", "tp"),
            P("ep", None),
            P("ep", None, "tp"),
            P("ep", None, "tp"),
            P("ep", "tp", None),
            P("tp", "ep"),
            P(),
        ),
        check_vma=False,
    )
```

profile of v0, /device:TPU:0, one launch (start us, length us, event | category | flops | bytes accessed | tf_op | source)
XLA Modules:
  0.0 121.8 jit_solution(18386872155913374480)
XLA Ops:
  0.7 0.8 fusion.46
  1.5 0.1 convolution_select_fusion
  1.7 0.1 bitcast_compare_fusion
  1.8 1.7 %convolution_convert_fusion.5 = bf16[320,256]{1,0:T(8,128)(2,1)} fusion(pred[320,128]{1,0:T(32,128)(4,1)S(1)} %bitcast_compare_fusion, bf16[128,256]{1,0:T(8,128)(2,1)} %param.9), kind=kOutput, calls=%fused_computation.20 | convolution fusion | flops 21053440 | bytes 270336 | tf_op jit(solution)/shard_map/dot_general | solution.py:47
  3.5 7.3 %all-to-all-start.1 = ((bf16[8,40,256]{2,1,0:T(8,128)(2,1)}), bf16[8,40,256]{2,1,0:T(8,128)(2,1)S(1)}, u32[]{:S(2)}, u32[]{:S(2)}) async-start(bf16[8,40,256]{2,1,0:T(8,128)(2,1)} %bitcast.6), calls=%async_computation.1 | async-start | bytes 327680 | tf_op jit(solution)/shard_map/all_to_all | solution.py:18
  10.8 0.7 convert_element_type.82
  11.4 0.7 select_reduce_fusion.1
  12.1 6.0 %all_gather.6 = bf16[128,1024]{1,0:T(8,128)(2,1)S(1)} all-gather(bf16[128,256]{1,0:T(8,128)(2,1)} %param.10), channel_id=1, replica_groups=mesh['ep'=8,'tp'=4] {'tp'}, dimensions={1}, use_global_device_ids=true | all-gather | bytes 327680 | tf_op jit(solution)/shard_map/all_gather | solution.py:51
  18.1 0.3 convolution_convert_fusion.3
  18.4 0.2 fusion.27
  18.6 0.9 pad_maximum_fusion.1
  19.5 6.1 %all-to-all-start = ((bf16[8,40,1152]{2,1,0:T(8,128)(2,1)}), bf16[8,40,1152]{2,1,0:T(8,128)(2,1)}, u32[]{:S(2)}, u32[]{:S(2)}) async-start(bf16[8,40,1152]{2,1,0:T(8,128)(2,1)} %pad_maximum_fusion.1), calls=%async_computation | async-start | bytes 1474560 | tf_op jit(solution)/shard_map/all_to_all | solution.py:18
  25.7 7.9 %all_gather.7 = bf16[320,1024]{1,0:T(8,128)(2,1)S(1)} all-gather(bf16[320,256]{1,0:T(8,128)(2,1)S(1)} %bitcast.83), channel_id=1, replica_groups=mesh['ep'=8,'tp'=4] {'tp'}, dimensions={1}, use_global_device_ids=true | all-gather | bytes 819200 | tf_op jit(solution)/shard_map/all_gather | solution.py:56
  33.6 1.7 %fusion.9 = f32[320,704]{1,0:T(8,128)} fusion(bf16[320,1024]{1,0:T(8,128)(2,1)S(1)} %all_gather.7, bf16[1,1024,704]{1,2,0:T(8,128)(2,1)S(1)} %copy-done.1), kind=kOutput, calls=%fused_computation.12 | convolution fusion | flops 461373440 | bytes 2998272 | tf_op jit(solution)/shard_map/dot_general | solution.py:72
  35.3 1.7 %fusion.5 = f32[320,704]{1,0:T(8,128)} fusion(bf16[320,1024]{1,0:T(8,128)(2,1)S(1)} %all_gather.7, bf16[1,1024,704]{1,2,0:T(8,128)(2,1)S(1)} %copy-done), kind=kOutput, calls=%fused_computation.8 | convolution fusion | flops 461373440 | bytes 2998272 | tf_op jit(solution)/shard_map/dot_general | solution.py:71
  37.0 8.4 %all-to-all-done = bf16[8,40,1152]{2,1,0:T(8,128)(2,1)} async-done(((bf16[8,40,1152]{2,1,0:T(8,128)(2,1)}), bf16[8,40,1152]{2,1,0:T(8,128)(2,1)}, u32[]{:S(2)}, u32[]{:S(2)}) %all-to-all-start) | async-done | bytes 737312 | tf_op jit(solution)/shard_map/all_to_all | solution.py:18
  45.4 1.0 convert_reduce_fusion.1
  46.4 3.3 %multiply_reduce_fusion.1 = (f32[320]{0:T(512)S(1)}, bf16[320,704]{1,0:T(8,128)(2,1)S(1)}, bf16[320,704]{1,0:T(8,128)(2,1)S(1)}) fusion(f32[320,704]{1,0:T(8,128)} %fusion.9, f32[320,704]{1,0:T(8,128)} %fusion.5, f32[320]{0:T(512)S(1)} %convert_reduce_fusion.1, bf16[1,704,1024]{2,1,0:T(8,128)(2,1)} %param.15, bf16[320,1152]{1,0:T(8,128)(2,1)} %bitcast.4), kind=kOutput, calls=%fused_computation.29 | convolution fusion | flops 465653440 | bytes 4966912 | tf_op jit(solution)/shard_map/dot_general | solution.py:77
  49.7 0.7 fusion.3
  50.4 0.1 copy-done.14
  50.5 0.2 copy-done.7
  50.6 0.7 fusion.16
  51.3 0.9 copy.45
  52.2 3.6 %all-to-all-start.2 = ((bf16[320,4,256]{2,0,1:T(8,128)(2,1)}), bf16[320,4,256]{2,0,1:T(8,128)(2,1)S(1)}, u32[]{:S(2)}, u32[]{:S(2)}) async-start(bf16[320,4,256]{2,0,1:T(8,128)(2,1)} %bitcast.76), calls=%async_computation.2 | async-start | bytes 1310720 | tf_op jit(solution)/shard_map/all_to_all | solution.py:89
  55.9 0.1 copy.37
  56.0 10.1 %all-to-all-done.2 = bf16[320,4,256]{2,0,1:T(8,128)(2,1)S(1)} async-done(((bf16[320,4,256]{2,0,1:T(8,128)(2,1)}), bf16[320,4,256]{2,0,1:T(8,128)(2,1)S(1)}, u32[]{:S(2)}, u32[]{:S(2)}) %all-to-all-start.2) | async-done | bytes 655392 | tf_op jit(solution)/shard_map/all_to_all | solution.py:89
  66.0 0.8 reduce_sum.95
  66.8 3.6 %all-to-all-start.3 = ((bf16[8,40,256]{2,1,0:T(8,128)(2,1)}), bf16[8,40,256]{2,1,0:T(8,128)(2,1)S(1)}, u32[]{:S(2)}, u32[]{:S(2)}) async-start(bf16[8,40,256]{2,1,0:T(8,128)(2,1)} %bitcast.10), calls=%async_computation.3 | async-start | bytes 327680 | tf_op jit(solution)/shard_map/all_to_all | solution.py:18
  70.5 0.3 convolution_convert_fusion.4
  70.9 1.1 pad_maximum_fusion
  71.9 6.1 %all-to-all-done.3 = bf16[8,40,256]{2,1,0:T(8,128)(2,1)S(1)} async-done(((bf16[8,40,256]{2,1,0:T(8,128)(2,1)}), bf16[8,40,256]{2,1,0:T(8,128)(2,1)S(1)}, u32[]{:S(2)}, u32[]{:S(2)}) %all-to-all-start.3) | async-done | bytes 163872 | tf_op jit(solution)/shard_map/all_to_all | solution.py:18
  78.0 0.7 copy-done.4
  78.7 3.6 %all-to-all-start.4 = ((bf16[8,512,128]{1,2,0:T(8,128)(2,1)}), bf16[8,512,128]{1,2,0:T(8,128)(2,1)S(1)}, u32[]{:S(2)}, u32[]{:S(2)}) async-start(bf16[8,512,128]{1,2,0:T(8,128)(2,1)} %pad_maximum_fusion), calls=%async_computation.4 | async-start | bytes 2097152 | tf_op jit(solution)/shard_map/all_to_all | solution.py:18
  82.2 1.4 %fusion.55 = f32[256,1024]{0,1:T(8,128)} fusion(bf16[128,256]{1,0:T(8,128)(2,1)S(1)} %copy-done.6, bf16[128,1024]{1,0:T(8,128)(2,1)S(1)} %all_gather.6), kind=kOutput, calls=%fused_computation.84 | convolution fusion | flops 67108864 | bytes 1376256 | tf_op jit(solution)/shard_map/reshape | solution.py:93
  83.6 3.2 %fusion = bf16[1,1024,704]{1,2,0:T(8,128)(2,1)} fusion(bf16[320,1024]{1,0:T(8,128)(2,1)S(1)} %copy-done.3, bf16[320,704]{1,0:T(8,128)(2,1)} %copy-done.14), kind=kOutput, calls=%fused_computation.3 | convolution fusion | flops 462094336 | bytes 2547712 | tf_op jit(solution)/shard_map/dot_general | solution.py:106
  86.8 2.1 %fusion.1 = bf16[1,1024,704]{1,2,0:T(8,128)(2,1)} fusion(bf16[320,1024]{1,0:T(8,128)(2,1)S(1)} %copy-done.3, bf16[320,704]{1,0:T(8,128)(2,1)S(1)} %copy-done.8), kind=kOutput, calls=%fused_computation.4 | convolution fusion | flops 462094336 | bytes 2547712 | tf_op jit(solution)/shard_map/dot_general | solution.py:107
  88.9 3.3 %fusion.2 = bf16[1,704,1024]{2,1,0:T(8,128)(2,1)} fusion(bf16[320,1152]{1,0:T(8,128)(2,1)} %bitcast.4, f32[320]{0:T(512)S(1)} %convert_reduce_fusion.1, f32[320,704]{1,0:T(8,128)S(1)} %copy-done.12, f32[320,704]{1,0:T(8,128)S(1)} %copy-done.13), kind=kOutput, calls=%fused_computation.5 | convolution fusion | flops 463671296 | bytes 3900672 | tf_op jit(solution)/shard_map/dot_general | solution.py:108
  92.2 0.3 convolution_bitcast_fusion
  92.5 14.3 %all-to-all-done.4 = bf16[8,512,128]{1,2,0:T(8,128)(2,1)S(1)} async-done(((bf16[8,512,128]{1,2,0:T(8,128)(2,1)}), bf16[8,512,128]{1,2,0:T(8,128)(2,1)S(1)}, u32[]{:S(2)}, u32[]{:S(2)}) %all-to-all-start.4) | async-done | bytes 1048608 | tf_op jit(solution)/shard_map/all_to_all | solution.py:18
  106.8 1.5 %convert_reduce_fusion = (f32[256,128]{0,1:T(8,128)S(1)}, f32[8,128]{1,0:T(8,128)S(1)}) fusion(bf16[8,512,128]{1,2,0:T(8,128)(2,1)S(1)} %all-to-all-done.4, f32[8,256,128]{1,2,0:T(8,128)} %bitcast.78), kind=kLoop, calls=%fused_computation.26 | loop fusion | flops 1276928 | bytes 2232320 | tf_op jit(solution)/shard_map/reduce_sum | solution.py:67
  108.4 0.8 broadcast_in_dim.108
  109.1 2.9 %all-to-all-start.5 = ((f32[32,1,1064]{2,1,0:T(1,128)}), f32[32,1,1064]{2,1,0:T(1,128)S(1)}, u32[]{:S(2)}, u32[]{:S(2)}) async-start(f32[32,1,1064]{2,1,0:T(1,128)} %broadcast_in_dim.108), calls=%async_computation.5 | async-start | bytes 294912 | tf_op jit(solution)/shard_map/all_to_all | solution.py:18
  112.1 0.8 copy.39
  112.9 0.9 fusion.19
  113.7 6.7 %all-to-all-done.5 = f32[32,1,1064]{2,1,0:T(1,128)S(1)} async-done(((f32[32,1,1064]{2,1,0:T(1,128)}), f32[32,1,1064]{2,1,0:T(1,128)S(1)}, u32[]{:S(2)}, u32[]{:S(2)}) %all-to-all-start.5) | async-done | bytes 136224 | tf_op jit(solution)/shard_map/all_to_all | solution.py:18
  120.5 0.1 fusion.29
  120.7 0.6 select_reduce_fusion
  121.2 0.6 broadcast_multiply_fusion.1
  (42 shorter events, 0.4 us)
Async XLA Ops:
  0.6 34.6 %copy-start = (bf16[1,1024,704]{1,2,0:T(8,128)(2,1)S(1)}, bf16[1,1024,704]{1,2,0:T(8,128)(2,1)}, u32[]{:S(2)}) copy-start(bf16[1,1024,704]{1,2,0:T(8,128)(2,1)} %param.13) | copy-start | bytes 4325380
  3.5 16.0 %all-to-all-start.1 = ((bf16[8,40,256]{2,1,0:T(8,128)(2,1)}), bf16[8,40,256]{2,1,0:T(8,128)(2,1)S(1)}, u32[]{:S(2)}, u32[]{:S(2)}) async-start(bf16[8,40,256]{2,1,0:T(8,128)(2,1)} %bitcast.6), calls=%async_computation.1 | async-start | bytes 327680 | tf_op jit(solution)/shard_map/all_to_all | solution.py:18
  19.5 14.0 %copy-start.1 = (bf16[1,1024,704]{1,2,0:T(8,128)(2,1)S(1)}, bf16[1,1024,704]{1,2,0:T(8,128)(2,1)}, u32[]{:S(2)}) copy-start(bf16[1,1024,704]{1,2,0:T(8,128)(2,1)} %param.14) | copy-start | bytes 4325380
  19.5 25.8 %all-to-all-start = ((bf16[8,40,1152]{2,1,0:T(8,128)(2,1)}), bf16[8,40,1152]{2,1,0:T(8,128)(2,1)}, u32[]{:S(2)}, u32[]{:S(2)}) async-start(bf16[8,40,1152]{2,1,0:T(8,128)(2,1)} %pad_maximum_fusion.1), calls=%async_computation | async-start | bytes 1474560 | tf_op jit(solution)/shard_map/all_to_all | solution.py:18
  33.6 1.7 %copy-start.2 = (bf16[320,1024]{1,0:T(8,128)(2,1)}, bf16[320,1024]{1,0:T(8,128)(2,1)S(1)}, u32[]{:S(2)}) copy-start(bf16[320,1024]{1,0:T(8,128)(2,1)S(1)} %all_gather.7) | copy-start | bytes 1966084
  49.7 0.8 copy-start.14
  49.7 1.0 copy-start.7
  51.3 4.5 %copy-start.9 = (bf16[256,128]{1,0:T(8,128)(2,1)S(1)}, bf16[256,128]{1,0:T(8,128)(2,1)}, u32[]{:S(2)}) copy-start(bf16[256,128]{1,0:T(8,128)(2,1)} %param.16) | copy-start | bytes 196612
  52.2 18.2 %copy-start.6 = (bf16[128,256]{1,0:T(8,128)(2,1)S(1)}, bf16[128,256]{1,0:T(8,128)(2,1)}, u32[]{:S(2)}) copy-start(bf16[128,256]{1,0:T(8,128)(2,1)} %param.9) | copy-start | bytes 196612
  52.2 18.2 %copy-start.10 = (f32[1024]{0:T(1024)S(1)}, f32[1024]{0:T(1024)}, u32[]{:S(2)}) copy-start(f32[1024]{0:T(1024)} %param.17) | copy-start | bytes 12292
  52.2 13.8 %all-to-all-start.2 = ((bf16[320,4,256]{2,0,1:T(8,128)(2,1)}), bf16[320,4,256]{2,0,1:T(8,128)(2,1)S(1)}, u32[]{:S(2)}, u32[]{:S(2)}) async-start(bf16[320,4,256]{2,0,1:T(8,128)(2,1)} %bitcast.76), calls=%async_computation.2 | async-start | bytes 1310720 | tf_op jit(solution)/shard_map/all_to_all | solution.py:89
  66.8 11.2 %all-to-all-start.3 = ((bf16[8,40,256]{2,1,0:T(8,128)(2,1)}), bf16[8,40,256]{2,1,0:T(8,128)(2,1)S(1)}, u32[]{:S(2)}, u32[]{:S(2)}) async-start(bf16[8,40,256]{2,1,0:T(8,128)(2,1)} %bitcast.10), calls=%async_computation.3 | async-start | bytes 327680 | tf_op jit(solution)/shard_map/all_to_all | solution.py:18
  71.9 11.7 %copy-start.3 = (bf16[320,1024]{1,0:T(8,128)(2,1)S(1)}, bf16[320,1024]{1,0:T(8,128)(2,1)}, u32[]{:S(2)}) copy-start(bf16[320,1024]{1,0:T(8,128)(2,1)} %copy-done.2) | copy-start | bytes 1966084
  78.0 0.7 copy-start.4
  78.7 28.1 %all-to-all-start.4 = ((bf16[8,512,128]{1,2,0:T(8,128)(2,1)}), bf16[8,512,128]{1,2,0:T(8,128)(2,1)S(1)}, u32[]{:S(2)}, u32[]{:S(2)}) async-start(bf16[8,512,128]{1,2,0:T(8,128)(2,1)} %pad_maximum_fusion), calls=%async_computation.4 | async-start | bytes 2097152 | tf_op jit(solution)/shard_map/all_to_all | solution.py:18
  83.6 3.2 %copy-start.8 = (bf16[320,704]{1,0:T(8,128)(2,1)S(1)}, bf16[320,704]{1,0:T(8,128)(2,1)}, u32[]{:S(2)}) copy-start(bf16[320,704]{1,0:T(8,128)(2,1)} %copy-done.7) | copy-start | bytes 1351684
  86.8 2.1 %copy-start.12 = (f32[320,704]{1,0:T(8,128)S(1)}, f32[320,704]{1,0:T(8,128)}, u32[]{:S(2)}) copy-start(f32[320,704]{1,0:T(8,128)} %fusion.9) | copy-start | bytes 2703364
  86.8 2.1 %copy-start.13 = (f32[320,704]{1,0:T(8,128)S(1)}, f32[320,704]{1,0:T(8,128)}, u32[]{:S(2)}) copy-start(f32[320,704]{1,0:T(8,128)} %fusion.5) | copy-start | bytes 2703364
  88.9 3.3 %copy-start.5 = (bf16[8,40,256]{2,1,0:T(8,128)(2,1)S(1)}, bf16[8,40,256]{2,1,0:T(8,128)(2,1)}, u32[]{:S(2)}) copy-start(bf16[8,40,256]{2,1,0:T(8,128)(2,1)} %copy-done.4) | copy-start | bytes 491524
  109.1 11.3 %all-to-all-start.5 = ((f32[32,1,1064]{2,1,0:T(1,128)}), f32[32,1,1064]{2,1,0:T(1,128)S(1)}, u32[]{:S(2)}, u32[]{:S(2)}) async-start(f32[32,1,1064]{2,1,0:T(1,128)} %broadcast_in_dim.108), calls=%async_computation.5 | async-start | bytes 294912 | tf_op jit(solution)/shard_map/all_to_all | solution.py:18
  112.0 8.6 %copy-start.11 = (s32[128,2]{0,1:T(2,128)S(1)}, s32[128,2]{0,1:T(2,128)}, u32[]{:S(2)}) copy-start(s32[128,2]{0,1:T(2,128)} %param.11) | copy-start | bytes 3076
where the time goes:
time: 123 us; the launch traced here: 122 us
  waiting for transfers between devices  45.5 us (37%)
  starting transfers between devices  27.1 us (22%)
  matrix products  21.6 us (18%)
  blocking collectives  13.9 us (11%)
  other arithmetic  9.05 us (7%)
  local copies, waits for them, and re-layouts  3.72 us (3%)
    all_to_all x5, waiting for transfers between devices, swap(): return lax.all_to_all(values, axis, split_axis=0, concat_axis=0, tiled=True)  35.5 us
    all_to_all x5, starting transfers between devices, swap(): return lax.all_to_all(values, axis, split_axis=0, concat_axis=0, tiled=True)  23.5 us
    all_to_all x1, waiting for transfers between devices, local(): lax.all_to_all(partial_value, 'tp', split_axis=1, concat_axis=0, tiled=True)  10.1 us
    all_gather x1, blocking collectives, local(): lax.all_gather(rows_part.reshape(rows_here, width_part), 'tp', axis=1, ti...  7.9 us
    all_gather x1, blocking collectives, local(): grads_full = lax.all_gather(cotangent, 'tp', axis=1, tiled=True)  5.97 us
    all_to_all x1, starting transfers between devices, local(): lax.all_to_all(partial_value, 'tp', split_axis=1, concat_axis=0, tiled=True)  3.61 us
    dot_general x1, matrix products, local(): lax.dot_general(weighted, grads_in, contract_rows, preferred_element_type...  3.32 us
    dot_general x1, matrix products, local(): lax.dot_general(grads_in, down_matrix, contract_cols, preferred_element_t...  3.28 us
  transfers between devices with their start and end apart: 6, of which 5 were waited for; matrix products, arithmetic and copies ran while one was open for 16% of the time, Pallas kernels for 0%

commit v1 on v0

--- a/solution.py
+++ b/solution.py
@@ -6,6 +6,19 @@
 FF = 2816
 BF = jnp.bfloat16
 F32 = jnp.float32
+
+
+def collect(array, axis, dim):
+    devices, place, rows = (lax.axis_size(axis), lax.axis_index(axis), array.shape[dim])
+    forward = [(i, (i + 1) % devices) for i in range(devices)]
+    out = jnp.zeros((*array.shape[:dim], devices * rows, *array.shape[dim + 1 :]), array.dtype)
+    held = array
+    for step in range(devices):
+        holder = (place - step) % devices
+        out = lax.dynamic_update_slice_in_dim(out, held, holder * rows, axis=dim)
+        if step < devices - 1:
+            held = lax.ppermute(held, axis, forward)
+    return out
 
 
 def spread(values, group_size):
@@ -53,7 +66,7 @@
     arrived = swap(jnp.concatenate([pick(grads_full), lanes], axis=2), "ep")
     arrived = arrived.reshape(rows_here, width + 128)
     grads_in, weight_col = (arrived[:, :width], arrived[:, width : width + 1].astype(F32))
-    rows_in = lax.all_gather(rows_part.reshape(rows_here, width_part), "tp", axis=1, tiled=True)
+    rows_in = collect(rows_part.reshape(rows_here, width_part), "tp", 1)
     contract_rows = (((0,), (0,)), ((), ()))
     contract_cols = (((1,), (1,)), ((), ()))
     dense_cols = dense_weight.shape[1]

time: 123 us -> 122 us (level)
  blocking collectives: 13.9 us -> 5.97 us
  waiting for transfers between devices: 45.5 us -> 53.3 us
  other arithmetic: 9.05 us -> 7.72 us
    ppermute x0 -> x3, waiting for transfers between devices: none -> 14 us  [collect(): held = lax.ppermute(held, axis, forward)]
    all_gather x1 -> x0, blocking collectives: 7.9 us -> none  [local(): lax.all_gather(rows_part.reshape(rows_here, width_part), 'tp', axis=1, ti...]
    all_to_all x5, waiting for transfers between devices: 35.5 us -> 29.2 us  [swap(): return lax.all_to_all(values, axis, split_axis=0, concat_axis=0, tiled=True)]
  transfers between devices with their start and end apart: 6 -> 9, of which waited for: 5 -> 9; matrix products, arithmetic and copies ran while one was open for 16% -> 15% of each run, Pallas kernels for 0% -> 0%
where the time goes in v1:
time: 122 us; the launch traced here: 121 us
  waiting for transfers between devices  53.3 us (44%)
  starting transfers between devices  27.3 us (22%)
  matrix products  21.6 us (18%)
  other arithmetic  7.72 us (6%)
  blocking collectives  5.97 us (5%)
  local copies, waits for them, and re-layouts  3.86 us (3%)
    all_to_all x5, waiting for transfers between devices, swap(): return lax.all_to_all(values, axis, split_axis=0, concat_axis=0, tiled=True)  29.2 us
    all_to_all x5, starting transfers between devices, swap(): return lax.all_to_all(values, axis, split_axis=0, concat_axis=0, tiled=True)  23.6 us
    ppermute x3, waiting for transfers between devices, collect(): held = lax.ppermute(held, axis, forward)  14 us
    all_to_all x1, waiting for transfers between devices, local(): lax.all_to_all(partial_value, 'tp', split_axis=1, concat_axis=0, tiled=True)  10.1 us
    all_gather x1, blocking collectives, local(): grads_full = lax.all_gather(cotangent, 'tp', axis=1, tiled=True)  5.97 us
    all_to_all x1, starting transfers between devices, local(): lax.all_to_all(partial_value, 'tp', split_axis=1, concat_axis=0, tiled=True)  3.61 us
    dot_general x1, matrix products, local(): lax.dot_general(weighted, grads_in, contract_rows, preferred_element_type...  3.32 us
    dot_general x1, matrix products, local(): lax.dot_general(grads_in, down_matrix, contract_cols, preferred_element_t...  3.28 us
  transfers between devices with their start and end apart: 9, of which 9 were waited for; matrix products, arithmetic and copies ran while one was open for 15% of the time, Pallas kernels for 0%

profile of v1, /device:TPU:0, one launch (start us, length us, event | category | flops | bytes accessed | tf_op | source)
XLA Modules:
  0.0 120.7 jit_solution(8492485326082151080)
XLA Ops:
  0.8 0.8 fusion.46
  1.5 0.1 convolution_select_fusion
  1.7 0.1 bitcast_compare_fusion
  1.8 1.7 %convolution_convert_fusion.5 = bf16[320,256]{1,0:T(8,128)(2,1)} fusion(pred[320,128]{1,0:T(32,128)(4,1)S(1)} %bitcast_compare_fusion, bf16[128,256]{1,0:T(8,128)(2,1)} %param.9), kind=kOutput, calls=%fused_computation.20 | convolution fusion | flops 21053440 | bytes 270336 | tf_op jit(solution)/shard_map/dot_general | solution.py:60
  3.5 7.3 %all-to-all-start.1 = ((bf16[8,40,256]{2,1,0:T(8,128)(2,1)}), bf16[8,40,256]{2,1,0:T(8,128)(2,1)S(1)}, u32[]{:S(2)}, u32[]{:S(2)}) async-start(bf16[8,40,256]{2,1,0:T(8,128)(2,1)} %bitcast.6), calls=%async_computation.1 | async-start | bytes 327680 | tf_op jit(solution)/shard_map/all_to_all | solution.py:31
  10.8 6.0 %all_gather.3 = bf16[128,1024]{1,0:T(8,128)(2,1)S(1)} all-gather(bf16[128,256]{1,0:T(8,128)(2,1)} %param.10), channel_id=1, replica_groups=mesh['ep'=8,'tp'=4] {'tp'}, dimensions={1}, use_global_device_ids=true | all-gather | bytes 327680 | tf_op jit(solution)/shard_map/all_gather | solution.py:64
  16.8 0.3 convolution_convert_fusion.3
  17.2 0.2 fusion.27
  17.3 0.9 pad_maximum_fusion.1
  18.3 0.1 all-to-all-done.1
  18.4 5.9 %all-to-all-start = ((bf16[8,40,1152]{2,1,0:T(8,128)(2,1)}), bf16[8,40,1152]{2,1,0:T(8,128)(2,1)}, u32[]{:S(2)}, u32[]{:S(2)}) async-start(bf16[8,40,1152]{2,1,0:T(8,128)(2,1)} %pad_maximum_fusion.1), calls=%async_computation | async-start | bytes 1474560 | tf_op jit(solution)/shard_map/all_to_all | solution.py:31
  24.3 4.7 %collective-permute-done = bf16[320,256]{1,0:T(8,128)(2,1)S(1)} collective-permute-done((bf16[320,256]{1,0:T(8,128)(2,1)S(1)}, bf16[320,256]{1,0:T(8,128)(2,1)S(1)}, u32[]{:S(2)}, u32[]{:S(2)}) %collective-permute-start) | collective-permute-done | bytes 163872 | tf_op jit(solution)/shard_map/ppermute | solution.py:20
  29.1 4.6 %collective-permute-done.1 = bf16[320,256]{1,0:T(8,128)(2,1)S(1)} collective-permute-done((bf16[320,256]{1,0:T(8,128)(2,1)S(1)}, bf16[320,256]{1,0:T(8,128)(2,1)S(1)}, u32[]{:S(2)}, u32[]{:S(2)}) %collective-permute-start.1) | collective-permute-done | bytes 163872 | tf_op jit(solution)/shard_map/ppermute | solution.py:20
  33.8 4.7 %collective-permute-done.2 = bf16[320,256]{1,0:T(8,128)(2,1)S(1)} collective-permute-done((bf16[320,256]{1,0:T(8,128)(2,1)S(1)}, bf16[320,256]{1,0:T(8,128)(2,1)S(1)}, u32[]{:S(2)}, u32[]{:S(2)}) %collective-permute-start.2) | collective-permute-done | bytes 163872 | tf_op jit(solution)/shard_map/ppermute | solution.py:20
  38.5 1.7 %fusion.5 = f32[320,704]{1,0:T(8,128)} fusion(bf16[320,1024]{1,0:T(8,128)(2,1)S(1)} %constant_dynamic-update-slice_fusion, bf16[1,1024,704]{1,2,0:T(8,128)(2,1)S(1)} %copy-done), kind=kOutput, calls=%fused_computation.8 | convolution fusion | flops 461373440 | bytes 2998272 | tf_op jit(solution)/shard_map/dot_general | solution.py:84
  40.2 1.7 %fusion.9 = f32[320,704]{1,0:T(8,128)} fusion(bf16[320,1024]{1,0:T(8,128)(2,1)S(1)} %constant_dynamic-update-slice_fusion, bf16[1,1024,704]{1,2,0:T(8,128)(2,1)S(1)} %copy-done.1), kind=kOutput, calls=%fused_computation.12 | convolution fusion | flops 461373440 | bytes 2998272 | tf_op jit(solution)/shard_map/dot_general | solution.py:85
  41.9 2.0 %all-to-all-done = bf16[8,40,1152]{2,1,0:T(8,128)(2,1)} async-done(((bf16[8,40,1152]{2,1,0:T(8,128)(2,1)}), bf16[8,40,1152]{2,1,0:T(8,128)(2,1)}, u32[]{:S(2)}, u32[]{:S(2)}) %all-to-all-start) | async-done | bytes 737312 | tf_op jit(solution)/shard_map/all_to_all | solution.py:31
  44.0 1.0 convert_reduce_fusion.1
  45.0 3.3 %multiply_reduce_fusion.1 = (f32[320]{0:T(512)S(1)}, bf16[320,704]{1,0:T(8,128)(2,1)S(1)}, bf16[320,704]{1,0:T(8,128)(2,1)S(1)}) fusion(f32[320,704]{1,0:T(8,128)} %fusion.9, f32[320,704]{1,0:T(8,128)} %fusion.5, f32[320]{0:T(512)S(1)} %convert_reduce_fusion.1, bf16[1,704,1024]{2,1,0:T(8,128)(2,1)} %param.15, bf16[320,1152]{1,0:T(8,128)(2,1)} %bitcast.4), kind=kOutput, calls=%fused_computation.29 | convolution fusion | flops 465653440 | bytes 4966912 | tf_op jit(solution)/shard_map/dot_general | solution.py:90
  48.3 0.7 fusion.3
  49.0 0.2 copy-done.7
  49.2 0.7 fusion.16
  49.9 0.9 copy.45
  50.8 3.6 %all-to-all-start.2 = ((bf16[320,4,256]{2,0,1:T(8,128)(2,1)}), bf16[320,4,256]{2,0,1:T(8,128)(2,1)S(1)}, u32[]{:S(2)}, u32[]{:S(2)}) async-start(bf16[320,4,256]{2,0,1:T(8,128)(2,1)} %bitcast.76), calls=%async_computation.2 | async-start | bytes 1310720 | tf_op jit(solution)/shard_map/all_to_all | solution.py:102
  54.5 0.1 copy.37
  54.6 10.1 %all-to-all-done.2 = bf16[320,4,256]{2,0,1:T(8,128)(2,1)S(1)} async-done(((bf16[320,4,256]{2,0,1:T(8,128)(2,1)}), bf16[320,4,256]{2,0,1:T(8,128)(2,1)S(1)}, u32[]{:S(2)}, u32[]{:S(2)}) %all-to-all-start.2) | async-done | bytes 655392 | tf_op jit(solution)/shard_map/all_to_all | solution.py:102
  64.6 0.8 reduce_sum.95
  65.4 4.0 %all-to-all-start.3 = ((bf16[8,40,256]{2,1,0:T(8,128)(2,1)}), bf16[8,40,256]{2,1,0:T(8,128)(2,1)S(1)}, u32[]{:S(2)}, u32[]{:S(2)}) async-start(bf16[8,40,256]{2,1,0:T(8,128)(2,1)} %bitcast.10), calls=%async_computation.3 | async-start | bytes 327680 | tf_op jit(solution)/shard_map/all_to_all | solution.py:31
  69.4 0.3 convolution_convert_fusion.4
  69.8 1.1 pad_maximum_fusion
  70.9 6.1 %all-to-all-done.3 = bf16[8,40,256]{2,1,0:T(8,128)(2,1)S(1)} async-done(((bf16[8,40,256]{2,1,0:T(8,128)(2,1)}), bf16[8,40,256]{2,1,0:T(8,128)(2,1)S(1)}, u32[]{:S(2)}, u32[]{:S(2)}) %all-to-all-start.3) | async-done | bytes 163872 | tf_op jit(solution)/shard_map/all_to_all | solution.py:31
  76.9 0.7 copy-done.4
  77.6 3.6 %all-to-all-start.4 = ((bf16[8,512,128]{1,2,0:T(8,128)(2,1)}), bf16[8,512,128]{1,2,0:T(8,128)(2,1)S(1)}, u32[]{:S(2)}, u32[]{:S(2)}) async-start(bf16[8,512,128]{1,2,0:T(8,128)(2,1)} %pad_maximum_fusion), calls=%async_computation.4 | async-start | bytes 2097152 | tf_op jit(solution)/shard_map/all_to_all | solution.py:31
  81.2 1.4 %fusion.55 = f32[256,1024]{0,1:T(8,128)} fusion(bf16[128,256]{1,0:T(8,128)(2,1)S(1)} %copy-done.6, bf16[128,1024]{1,0:T(8,128)(2,1)S(1)} %all_gather.3), kind=kOutput, calls=%fused_computation.88 | convolution fusion | flops 67108864 | bytes 1376256 | tf_op jit(solution)/shard_map/reshape | solution.py:106
  82.5 3.2 %fusion = bf16[1,1024,704]{1,2,0:T(8,128)(2,1)} fusion(bf16[320,1024]{1,0:T(8,128)(2,1)S(1)} %copy-done.3, bf16[320,704]{1,0:T(8,128)(2,1)} %copy-done.15), kind=kOutput, calls=%fused_computation.3 | convolution fusion | flops 462094336 | bytes 2547712 | tf_op jit(solution)/shard_map/dot_general | solution.py:119
  85.7 2.1 %fusion.1 = bf16[1,1024,704]{1,2,0:T(8,128)(2,1)} fusion(bf16[320,1024]{1,0:T(8,128)(2,1)S(1)} %copy-done.3, bf16[320,704]{1,0:T(8,128)(2,1)S(1)} %copy-done.8), kind=kOutput, calls=%fused_computation.4 | convolution fusion | flops 462094336 | bytes 2547712 | tf_op jit(solution)/shard_map/dot_general | solution.py:120
  87.8 3.3 %fusion.2 = bf16[1,704,1024]{2,1,0:T(8,128)(2,1)} fusion(bf16[320,1152]{1,0:T(8,128)(2,1)} %bitcast.4, f32[320]{0:T(512)S(1)} %convert_reduce_fusion.1, f32[320,704]{1,0:T(8,128)S(1)} %copy-done.14, f32[320,704]{1,0:T(8,128)S(1)} %copy-done.13), kind=kOutput, calls=%fused_computation.5 | convolution fusion | flops 463671296 | bytes 3900672 | tf_op jit(solution)/shard_map/dot_general | solution.py:121
  91.1 0.3 convolution_bitcast_fusion
  91.4 14.3 %all-to-all-done.4 = bf16[8,512,128]{1,2,0:T(8,128)(2,1)S(1)} async-done(((bf16[8,512,128]{1,2,0:T(8,128)(2,1)}), bf16[8,512,128]{1,2,0:T(8,128)(2,1)S(1)}, u32[]{:S(2)}, u32[]{:S(2)}) %all-to-all-start.4) | async-done | bytes 1048608 | tf_op jit(solution)/shard_map/all_to_all | solution.py:31
  105.7 1.5 %convert_reduce_fusion = (f32[256,128]{0,1:T(8,128)S(1)}, f32[8,128]{1,0:T(8,128)S(1)}) fusion(bf16[8,512,128]{1,2,0:T(8,128)(2,1)S(1)} %all-to-all-done.4, f32[8,256,128]{1,2,0:T(8,128)} %bitcast.78), kind=kLoop, calls=%fused_computation.26 | loop fusion | flops 1276928 | bytes 2232320 | tf_op jit(solution)/shard_map/reduce_sum | solution.py:80
  107.3 0.8 broadcast_in_dim.112
  108.0 2.9 %all-to-all-start.5 = ((f32[32,1,1064]{2,1,0:T(1,128)}), f32[32,1,1064]{2,1,0:T(1,128)S(1)}, u32[]{:S(2)}, u32[]{:S(2)}) async-start(f32[32,1,1064]{2,1,0:T(1,128)} %broadcast_in_dim.112), calls=%async_computation.5 | async-start | bytes 294912 | tf_op jit(solution)/shard_map/all_to_all | solution.py:31
  111.0 0.8 copy.39
  111.8 0.9 fusion.19
  112.6 6.7 %all-to-all-done.5 = f32[32,1,1064]{2,1,0:T(1,128)S(1)} async-done(((f32[32,1,1064]{2,1,0:T(1,128)}), f32[32,1,1064]{2,1,0:T(1,128)S(1)}, u32[]{:S(2)}, u32[]{:S(2)}) %all-to-all-start.5) | async-done | bytes 136224 | tf_op jit(solution)/shard_map/all_to_all | solution.py:31
  119.4 0.1 fusion.29
  119.6 0.6 select_reduce_fusion
  120.1 0.6 broadcast_multiply_fusion.1
  (54 shorter events, 0.7 us)
Async XLA Ops:
  0.6 37.9 %copy-start = (bf16[1,1024,704]{1,2,0:T(8,128)(2,1)S(1)}, bf16[1,1024,704]{1,2,0:T(8,128)(2,1)}, u32[]{:S(2)}) copy-start(bf16[1,1024,704]{1,2,0:T(8,128)(2,1)} %param.13) | copy-start | bytes 4325380
  0.6 16.5 %copy-start.11 = (s32[128,2]{0,1:T(2,128)S(1)}, s32[128,2]{0,1:T(2,128)}, u32[]{:S(2)}) copy-start(s32[128,2]{0,1:T(2,128)} %param.11) | copy-start | bytes 3076
  0.7 16.4 %copy-start.12 = (bf16[128,2]{0,1:T(2,128)(2,1)S(1)}, bf16[128,2]{0,1:T(2,128)(2,1)}, u32[]{:S(2)}) copy-start(bf16[128,2]{0,1:T(2,128)(2,1)} %param.12) | copy-start | bytes 1540
  3.5 14.8 %all-to-all-start.1 = ((bf16[8,40,256]{2,1,0:T(8,128)(2,1)}), bf16[8,40,256]{2,1,0:T(8,128)(2,1)S(1)}, u32[]{:S(2)}, u32[]{:S(2)}) async-start(bf16[8,40,256]{2,1,0:T(8,128)(2,1)} %bitcast.6), calls=%async_computation.1 | async-start | bytes 327680 | tf_op jit(solution)/shard_map/all_to_all | solution.py:31
  18.4 25.6 %all-to-all-start = ((bf16[8,40,1152]{2,1,0:T(8,128)(2,1)}), bf16[8,40,1152]{2,1,0:T(8,128)(2,1)}, u32[]{:S(2)}, u32[]{:S(2)}) async-start(bf16[8,40,1152]{2,1,0:T(8,128)(2,1)} %pad_maximum_fusion.1), calls=%async_computation | async-start | bytes 1474560 | tf_op jit(solution)/shard_map/all_to_all | solution.py:31
  24.3 4.7 %collective-permute-start = (bf16[320,256]{1,0:T(8,128)(2,1)S(1)}, bf16[320,256]{1,0:T(8,128)(2,1)S(1)}, u32[]{:S(2)}, u32[]{:S(2)}) collective-permute-start(bf16[320,256]{1,0:T(8,128)(2,1)S(1)} %bitcast.83), channel_id=1, source_target_pairs={{0,1},{1,2},{2,3},{3,0},{4,5},{5,6},{6,7},{7,4},{8,9},{9,10},{10,1... | collective-permute-start | bytes 491528 | tf_op jit(solution)/shard_map/ppermute | solution.py:20
  29.0 4.7 %collective-permute-start.1 = (bf16[320,256]{1,0:T(8,128)(2,1)S(1)}, bf16[320,256]{1,0:T(8,128)(2,1)S(1)}, u32[]{:S(2)}, u32[]{:S(2)}) collective-permute-start(bf16[320,256]{1,0:T(8,128)(2,1)S(1)} %collective-permute-done), channel_id=1, source_target_pairs={{0,1},{1,2},{2,3},{3,0},{4,5},{5,6},{6,7},{7,4},{8,9},{9,10},{10,1... | collective-permute-start | bytes 491528 | tf_op jit(solution)/shard_map/ppermute | solution.py:20
  33.7 4.7 %collective-permute-start.2 = (bf16[320,256]{1,0:T(8,128)(2,1)S(1)}, bf16[320,256]{1,0:T(8,128)(2,1)S(1)}, u32[]{:S(2)}, u32[]{:S(2)}) collective-permute-start(bf16[320,256]{1,0:T(8,128)(2,1)S(1)} %collective-permute-done.1), channel_id=1, source_target_pairs={{0,1},{1,2},{2,3},{3,0},{4,5},{5,6},{6,7},{7,4},{8,9},{9,10},{10,1... | collective-permute-start | bytes 491528 | tf_op jit(solution)/shard_map/ppermute | solution.py:20
  38.5 1.7 %copy-start.2 = (bf16[320,1024]{1,0:T(8,128)(2,1)}, bf16[320,1024]{1,0:T(8,128)(2,1)S(1)}, u32[]{:S(2)}) copy-start(bf16[320,1024]{1,0:T(8,128)(2,1)S(1)} %constant_dynamic-update-slice_fusion) | copy-start | bytes 1966084
  38.5 1.7 %copy-start.1 = (bf16[1,1024,704]{1,2,0:T(8,128)(2,1)S(1)}, bf16[1,1024,704]{1,2,0:T(8,128)(2,1)}, u32[]{:S(2)}) copy-start(bf16[1,1024,704]{1,2,0:T(8,128)(2,1)} %param.14) | copy-start | bytes 4325380
  48.3 0.8 copy-start.15
  48.3 1.0 copy-start.7
  49.9 4.5 %copy-start.9 = (bf16[256,128]{1,0:T(8,128)(2,1)S(1)}, bf16[256,128]{1,0:T(8,128)(2,1)}, u32[]{:S(2)}) copy-start(bf16[256,128]{1,0:T(8,128)(2,1)} %param.16) | copy-start | bytes 196612
  50.8 18.6 %copy-start.6 = (bf16[128,256]{1,0:T(8,128)(2,1)S(1)}, bf16[128,256]{1,0:T(8,128)(2,1)}, u32[]{:S(2)}) copy-start(bf16[128,256]{1,0:T(8,128)(2,1)} %param.9) | copy-start | bytes 196612
  50.8 18.6 %copy-start.10 = (f32[1024]{0:T(1024)S(1)}, f32[1024]{0:T(1024)}, u32[]{:S(2)}) copy-start(f32[1024]{0:T(1024)} %param.17) | copy-start | bytes 12292
  50.8 13.8 %all-to-all-start.2 = ((bf16[320,4,256]{2,0,1:T(8,128)(2,1)}), bf16[320,4,256]{2,0,1:T(8,128)(2,1)S(1)}, u32[]{:S(2)}, u32[]{:S(2)}) async-start(bf16[320,4,256]{2,0,1:T(8,128)(2,1)} %bitcast.76), calls=%async_computation.2 | async-start | bytes 1310720 | tf_op jit(solution)/shard_map/all_to_all | solution.py:102
  65.4 11.5 %all-to-all-start.3 = ((bf16[8,40,256]{2,1,0:T(8,128)(2,1)}), bf16[8,40,256]{2,1,0:T(8,128)(2,1)S(1)}, u32[]{:S(2)}, u32[]{:S(2)}) async-start(bf16[8,40,256]{2,1,0:T(8,128)(2,1)} %bitcast.10), calls=%async_computation.3 | async-start | bytes 327680 | tf_op jit(solution)/shard_map/all_to_all | solution.py:31
  70.9 11.7 %copy-start.3 = (bf16[320,1024]{1,0:T(8,128)(2,1)S(1)}, bf16[320,1024]{1,0:T(8,128)(2,1)}, u32[]{:S(2)}) copy-start(bf16[320,1024]{1,0:T(8,128)(2,1)} %copy-done.2) | copy-start | bytes 1966084
  76.9 0.7 copy-start.4
  77.6 28.1 %all-to-all-start.4 = ((bf16[8,512,128]{1,2,0:T(8,128)(2,1)}), bf16[8,512,128]{1,2,0:T(8,128)(2,1)S(1)}, u32[]{:S(2)}, u32[]{:S(2)}) async-start(bf16[8,512,128]{1,2,0:T(8,128)(2,1)} %pad_maximum_fusion), calls=%async_computation.4 | async-start | bytes 2097152 | tf_op jit(solution)/shard_map/all_to_all | solution.py:31
  82.5 3.2 %copy-start.8 = (bf16[320,704]{1,0:T(8,128)(2,1)S(1)}, bf16[320,704]{1,0:T(8,128)(2,1)}, u32[]{:S(2)}) copy-start(bf16[320,704]{1,0:T(8,128)(2,1)} %copy-done.7) | copy-start | bytes 1351684
  85.7 2.1 %copy-start.13 = (f32[320,704]{1,0:T(8,128)S(1)}, f32[320,704]{1,0:T(8,128)}, u32[]{:S(2)}) copy-start(f32[320,704]{1,0:T(8,128)} %fusion.5) | copy-start | bytes 2703364
  85.7 2.1 %copy-start.14 = (f32[320,704]{1,0:T(8,128)S(1)}, f32[320,704]{1,0:T(8,128)}, u32[]{:S(2)}) copy-start(f32[320,704]{1,0:T(8,128)} %fusion.9) | copy-start | bytes 2703364
  87.8 3.3 %copy-start.5 = (bf16[8,40,256]{2,1,0:T(8,128)(2,1)S(1)}, bf16[8,40,256]{2,1,0:T(8,128)(2,1)}, u32[]{:S(2)}) copy-start(bf16[8,40,256]{2,1,0:T(8,128)(2,1)} %copy-done.4) | copy-start | bytes 491524
  108.0 11.3 %all-to-all-start.5 = ((f32[32,1,1064]{2,1,0:T(1,128)}), f32[32,1,1064]{2,1,0:T(1,128)S(1)}, u32[]{:S(2)}, u32[]{:S(2)}) async-start(f32[32,1,1064]{2,1,0:T(1,128)} %broadcast_in_dim.112), calls=%async_computation.5 | async-start | bytes 294912 | tf_op jit(solution)/shard_map/all_to_all | solution.py:31
